TPU v7x, 32 devices: a whole 2x2x4 slice. The times are simulated.
32 devices in a mesh: ep: 8 (over z, x), tp: 4 (over y, core).
Axes of the slice: x: 2, y: 2, z: 4, core: 2. Of those that a mesh axis runs over, the one named last changes fastest.
Arguments:
- queries: bfloat16 [4096, 2048], P('ep', 'tp'), may hold values from -5 to 5
- key_rows: bfloat16 [4096, 2048], P('ep', 'tp'), may hold values from -5 to 5
- values: bfloat16 [4096, 2048], P('ep', 'tp'), may hold values from -6 to 6
- forget_log: float32 [4096, 16], P(None, 'tp'), may hold values from -515 to 0, as said below
- out_weight: bfloat16 [2048, 4096], P(None, 'tp'), may hold values from -1 to 1
- expert_input: bfloat16 [1024, 4096], P(('ep', 'tp')), may hold values from -6 to 6
- norm_gain: float32 [4096], replicated, may hold values from 0.1 to 1.9
- route_ids: int32 [1024, 2], P('ep'), may hold values from 0 to 7, all different within a row; in each aligned block of 128 rows (0 to 127, 128 to 255, ...) at most 64 rows name the same one
- route_weights: float32 [1024, 2], P('ep'), may hold values from 0.2 to 1
- gate_weight: bfloat16 [8, 4096, 2048], P('ep', None, 'tp'), may hold values from -0.09375 to 0.09375
- up_weight: bfloat16 [8, 4096, 2048], P('ep', None, 'tp'), may hold values from -0.09375 to 0.09375
- down_weight: bfloat16 [8, 2048, 4096], P('ep', None, 'tp'), may hold values from -0.125 to 0.125
Outputs:
- mixer_out: bfloat16 [4096, 4096], P('ep', 'tp')
- expert_out: bfloat16 [1024, 4096], P('ep', 'tp')
Inputs may be any that keep to these rules, and one draw needn't show every extreme that they name: forget_log[t, h] is the sum of the log forget gates of head h at positions 0 to t of the one sequence; it never rises along positions. `route_ids`: each row names 2 different experts. In each aligned block of 128 rows (the rows of one index of ep) no expert is named by more than 64 rows, and some block reaches 64.
All inputs are finite; a program needn't handle non-finite values.
Results may differ from a plain program's by a relative error of at most 0.0071.
Values may be sent and summed in bfloat16 or wider, within the bound.
A program may use at most 64 MiB of HBM per device.

v0:
```python
import jax
import jax.numpy as jnp
from jax import lax
from jax.sharding import PartitionSpec as P

EPSILON = 1e-05


def slot_places(route_rows, experts, capacity):
    entries = route_rows.reshape(-1)
    matches = (entries[:, None] == jnp.arange(experts, dtype=jnp.int32)[None, :]).astype(jnp.int32)
    earlier = jnp.cumsum(matches, axis=0) - matches
    ranking = jnp.sum(earlier * matches, axis=1)
    return entries * capacity + ranking


def source_table(places, rows_count, chosen, total_slots):
    owners = jnp.arange(places.shape[0], dtype=jnp.int32) // chosen
    return jnp.full((total_slots,), rows_count, jnp.int32).at[places].set(owners)


def body(
    queries,
    key_rows,
    values,
    forget_log,
    out_weight,
    expert_input,
    norm_gain,
    route_ids,
    route_weights,
    gate_weight,
    up_weight,
    down_weight,
):
    row_count = queries.shape[0]
    heads_here = forget_log.shape[1]
    head_width = queries.shape[1] // heads_here
    own_start = lax.axis_index("ep") * row_count
    position_indices = own_start + jnp.arange(row_count, dtype=jnp.int32)
    query_heads = queries.reshape(row_count, heads_here, head_width)
    query_gate = lax.dynamic_slice_in_dim(forget_log, own_start, row_count, 0)
    score_scale = head_width ** (-0.5)

    def fold_shard(state_now, shard_item):
        first_row, key_shard, value_shard = shard_item

        def attend(state_in):
            row_max, row_total, weighted = state_in
            key_heads = key_shard.reshape(row_count, heads_here, head_width)
            value_heads = value_shard.reshape(row_count, heads_here, head_width)
            key_gate = lax.dynamic_slice_in_dim(forget_log, first_row, row_count, 0)
            scores = (
                jnp.einsum(
                    "qhd,khd->hqk", query_heads, key_heads, preferred_element_type=jnp.float32
                )
                * score_scale
            )
            scores = scores + query_gate.T[:, :, None] - key_gate.T[:, None, :]
            key_pos = first_row + jnp.arange(row_count, dtype=jnp.int32)
            scores = jnp.where(
                key_pos[None, None, :] <= position_indices[None, :, None], scores, -jnp.inf
            )
            newest = jnp.maximum(row_max, jnp.max(scores, axis=2))
            factor = jnp.exp(row_max - newest)
            weights_now = jnp.exp(scores - newest[:, :, None])
            row_total = row_total * factor + jnp.sum(weights_now, axis=2)
            weighted = weighted * factor[:, :, None] + jnp.einsum(
                "hqk,khd->hqd",
                weights_now.astype(jnp.bfloat16),
                value_heads,
                preferred_element_type=jnp.float32,
            )
            return (newest, row_total, weighted)

        return (
            lax.cond(first_row <= own_start, attend, lambda state_in: state_in, state_now),
            None,
        )

    initial = (
        jnp.full((heads_here, row_count), -jnp.inf, jnp.float32),
        jnp.zeros((heads_here, row_count), jnp.float32),
        jnp.zeros((heads_here, row_count, head_width), jnp.float32),
    )
    state_now = initial
    key_piece = lax.all_gather(key_rows, "ep", axis=0, tiled=True)
    value_piece = lax.all_gather(values, "ep", axis=0, tiled=True)
    shards = key_piece.shape[0] // row_count
    starts = row_count * jnp.arange(shards, dtype=jnp.int32)
    stacked = (
        starts,
        key_piece.reshape(shards, row_count, -1),
        value_piece.reshape(shards, row_count, -1),
    )
    state_now, _ = lax.scan(fold_shard, state_now, stacked)
    row_max, row_total, weighted = state_now
    attended = (
        (weighted / row_total[:, :, None])
        .transpose(1, 0, 2)
        .reshape(row_count, heads_here * head_width)
        .astype(jnp.bfloat16)
    )
    as_float = expert_input.astype(jnp.float32)
    center = jnp.mean(as_float, axis=1, keepdims=True)
    variance = jnp.mean(jnp.square(as_float - center), axis=1, keepdims=True)
    normed = ((as_float - center) * lax.rsqrt(variance + EPSILON) * norm_gain).astype(jnp.bfloat16)
    group_rows = lax.all_gather(normed, "tp", axis=0, tiled=True)
    block_rows = route_ids.shape[0]
    chosen = route_ids.shape[1]
    expert_local = gate_weight.shape[0]
    ep_count = lax.axis_size("ep")
    tp_count = lax.axis_size("tp")
    experts = expert_local * ep_count
    capacity = block_rows * chosen * 2 // experts
    places = slot_places(route_ids, experts, capacity)
    slot_table = source_table(places, block_rows, chosen, experts * capacity).reshape(
        ep_count, expert_local, capacity
    )
    share_size = capacity // tp_count
    part_table = lax.dynamic_slice_in_dim(
        slot_table, lax.axis_index("tp") * share_size, share_size, 2
    )
    outgoing = jnp.take(group_rows, part_table, axis=0, mode="fill", fill_value=0)
    arrived = lax.all_to_all(outgoing, "ep", split_axis=0, concat_axis=0, tiled=True)
    arrived_rows = lax.all_gather(arrived, "tp", axis=2, tiled=True)
    gate_part = jnp.einsum(
        "sxcd,xdf->sxcf", arrived_rows, gate_weight, preferred_element_type=jnp.float32
    )
    up_part = jnp.einsum(
        "sxcd,xdf->sxcf", arrived_rows, up_weight, preferred_element_type=jnp.float32
    )
    hidden = (jax.nn.silu(gate_part) * up_part).astype(jnp.bfloat16)
    slots_all = ep_count * expert_local * capacity
    flat_hidden = hidden.reshape(slots_all, hidden.shape[3])
    out_width = out_weight.shape[1]
    mixer_sum = jnp.dot(
        lax.all_gather(attended, "tp", axis=1, tiled=True),
        out_weight,
        preferred_element_type=jnp.float32,
    )
    part_rows = lax.all_gather(flat_hidden, "tp", axis=1, tiled=True)
    shaped = part_rows.reshape(ep_count, expert_local, capacity, part_rows.shape[1])
    product = jnp.einsum("sxcf,xfd->sxcd", shaped, down_weight, preferred_element_type=jnp.float32)
    expert_sum = product.reshape(slots_all, out_width)
    leaving = expert_sum.astype(jnp.bfloat16).reshape(ep_count, expert_local, capacity, out_width)
    returned = lax.all_to_all(leaving, "ep", split_axis=0, concat_axis=0, tiled=True)
    picked = jnp.take(returned.reshape(experts * capacity, out_width), places, axis=0).astype(
        jnp.float32
    )
    combined = jnp.sum(
        (picked * route_weights.reshape(-1)[:, None]).reshape(block_rows, chosen, out_width), axis=1
    )
    return (mixer_sum.astype(jnp.bfloat16), combined.astype(jnp.bfloat16))


def solution(mesh):
    placed = (
        P("ep", "tp"),
        P("ep", "tp"),
        P("ep", "tp"),
        P(None, "tp"),
        P(None, "tp"),
        P(("ep", "tp"), None),
        P(),
        P("ep", None),
        P("ep", None),
        P("ep", None, "tp"),
        P("ep", None, "tp"),
        P("ep", None, "tp"),
    )
    return jax.shard_map(
        body, mesh=mesh, in_specs=placed, out_specs=(P("ep", "tp"), P("ep", "tp")), check_vma=False
    )
```

profile of v0, /device:TPU:0, one launch (start us, length us, event | category | flops | bytes accessed | tf_op | source)
XLA Modules:
  0.0 390.9 jit_solution(14663094674887229282)
XLA Ops:
  7.2 1.1 convert_reduce_fusion
  8.3 1.2 fusion.49
  9.5 1.8 fusion.51
  11.4 0.8 copy.62
  12.5 0.7 broadcast_multiply_fusion
  13.4 0.6 reduce-window.6
  14.4 1.4 scatter_custom_fusion
  16.0 14.9 %all-gather.13.cloned.1.call-done = bf16[128,4096]{1,0:T(8,128)(2,1)} async-done(((bf16[32,4096]{1,0:T(8,128)(2,1)}), bf16[128,4096]{1,0:T(8,128)(2,1)}) %all-gather.13.cloned.1.call-update) | async-done | bytes 1048592 | tf_op jit(solution)/shard_map/all_gather | solution.py:108
  30.9 3.6 gather_fusion
  34.6 31.5 %all_to_all.10 = bf16[8,1,16,4096]{3,2,1,0:T(8,128)(2,1)} all-to-all(bf16[8,1,16,4096]{3,2,1,0:T(8,128)(2,1)S(1)} %broadcast_select_fusion), channel_id=1, replica_groups=mesh['ep'=8,'tp'=4] {'ep'}, dimensions={0} | all-to-all | bytes 2097152 | tf_op jit(solution)/shard_map/all_to_all | solution.py:125
  66.2 0.7 all-gather.7.cloned.1.call-update
  67.0 0.5 all-gather.9.cloned.1.call-update
  67.6 31.4 %all-gather.15.cloned.1.call-done = bf16[8,1,64,4096]{3,2,0,1:T(8,128)(2,1)} async-done(((bf16[8,1,16,4096]{3,2,0,1:T(8,128)(2,1)}), bf16[8,1,64,4096]{3,2,0,1:T(8,128)(2,1)}) %all-gather.15.cloned.1.call-update) | async-done | bytes 4194320 | tf_op jit(solution)/shard_map/all_gather | solution.py:126
  98.9 5.9 %fusion.27 = f32[8,1,64,512]{3,2,0,1:T(8,128)S(1)} fusion(bf16[1,4096,512]{2,1,0:T(8,128)(2,1)} %param.25, bf16[8,1,64,4096]{3,2,0,1:T(8,128)(2,1)} %all-gather.15.cloned.1.call-done), kind=kOutput, calls=%fused_computation.33 | convolution fusion | flops 2147483648 | bytes 9437184 | tf_op jit(solution)/shard_map/sxcd,xdf->sxcf/dot_general | solution.py:127
  104.9 3.2 fusion.42
  108.1 0.2 all-gather.11.cloned.1.call-start
  108.6 0.3 copy.59
  108.9 0.7 constant_dynamic-slice_fusion.2
  109.6 64.3 %all-gather.7.cloned.1.call-done = bf16[4096,512]{1,0:T(8,128)(2,1)} async-done(((bf16[512,512]{1,0:T(8,128)(2,1)}), bf16[4096,512]{1,0:T(8,128)(2,1)}) %all-gather.7.cloned.1.call-update) | async-done | bytes 4194320 | tf_op jit(solution)/shard_map/all_gather | solution.py:87
  173.9 6.5 %copy.58 = bf16[8,512,512]{1,2,0:T(8,128)(2,1)} copy(bf16[8,512,512]{2,1,0:T(8,128)(2,1)} %bitcast.117) | data formatting | bytes 8388608
  180.3 66.9 %all-gather.9.cloned.1.call-done = bf16[4096,512]{1,0:T(8,128)(2,1)} async-done(((bf16[512,512]{1,0:T(8,128)(2,1)}), bf16[4096,512]{1,0:T(8,128)(2,1)}) %all-gather.9.cloned.1.call-update) | async-done | bytes 4194320 | tf_op jit(solution)/shard_map/all_gather | solution.py:88
  247.2 6.5 %copy.60 = bf16[8,512,512]{1,2,0:T(8,128)(2,1)} copy(bf16[8,512,512]{2,1,0:T(8,128)(2,1)} %bitcast.118) | data formatting | bytes 8388608
  253.8 20.4 %while.16 = (s32[]{:T(128)}, f32[4,512]{1,0:T(4,128)S(1)}, f32[4,512]{1,0:T(4,128)S(1)}, f32[4,512,128]{2,1,0:T(8,128)S(1)}, s32[8]{0:T(128)S(1)}, /*index=5*/s3...) while((s32[]{:T(128)}, f32[4,512]{1,0:T(4,128)S(1)}, ...), condition=%wide.region_5.6_spmd.clone.clone, body=%wide.region_0.5_spmd.clone.clone.sunk | while | flops 555488256 | bytes 19607904 | solution.py:96
  253.8 0.6 dynamic_slice.43
  255.1 10.0 %conditional.4 = ((f32[4,512]{1,0:T(4,128)S(1)}, f32[4,512]{1,0:T(4,128)S(1)}, f32[4,512,128]{2,1,0:T(8,128)S(1)})) conditional(s32[]{:T(128)} %convert_element_type.100, (f32[4,512]{1,0:T(4,128)S(1)}, f32[4,512]{1,0:T(4,128)S(1)}, f32[4,512,128]{2,1,0:T(8,128)S(1)}) %tuple.54, (s32[]{:T(128)}, s32[]{:T(128)}, bf16[8,512,512]{1,2,0:T(8,128)(2,1)}, ...), branch_computations={%region_1.1_spmd, %region_2.4_spmd} | conditional | flops 555488256 | bytes 19605586 | solution.py:77
  257.0 0.8 dynamic-slice_bitcast_fusion
  257.8 0.6 iota_add_fusion
  258.4 0.2 broadcast_compare_fusion
  258.7 1.3 constant_dynamic-slice_fusion
  259.9 1.4 fusion.4
  261.4 1.4 fusion.3
  262.8 2.3 fusion.8
  265.1 0.6 dynamic_slice.43
  266.4 0.6 dynamic_slice.43
  267.7 0.6 dynamic_slice.43
  269.0 0.6 dynamic_slice.43
  270.3 0.6 dynamic_slice.43
  271.6 0.6 dynamic_slice.43
  272.9 0.6 dynamic_slice.43
  274.2 0.3 copy.61
  274.5 0.9 divide_convert_fusion
  275.5 6.1 %fusion.24 = bf16[8,1,64,1024]{3,2,1,0:T(8,128)(2,1)} fusion(bf16[8,64,2048]{2,1,0:T(8,128)(2,1)} %bitcast.129, bf16[1,2048,1024]{2,1,0:T(8,128)(2,1)} %param.27), kind=kOutput, calls=%fused_computation.32 | convolution fusion | flops 2148007936 | bytes 7340032 | tf_op jit(solution)/shard_map/sxcf,xfd->sxcd/dot_general | solution.py:144
  281.7 72.9 %all-to-all-start.1 = ((bf16[8,1,64,1024]{3,2,1,0:T(8,128)(2,1)}), bf16[8,1,64,1024]{3,2,1,0:T(8,128)(2,1)S(1)}, u32[]{:S(2)}, u32[]{:S(2)}) async-start(bf16[8,1,64,1024]{3,2,1,0:T(8,128)(2,1)} %fusion.24), calls=%async_computation.1 | async-start | bytes 2097152 | tf_op jit(solution)/shard_map/all_to_all | solution.py:147
  355.1 11.4 %all-gather.11.cloned.1.call-done = bf16[512,2048]{0,1:T(8,128)(2,1)} async-done(((bf16[512,512]{0,1:T(8,128)(2,1)}), bf16[512,2048]{0,1:T(8,128)(2,1)}) %all-gather.11.cloned.1.call-update) | async-done | bytes 2097168 | tf_op jit(solution)/shard_map/all_gather | solution.py:138
  366.5 6.1 %convolution_convert_fusion = bf16[512,1024]{1,0:T(8,128)(2,1)} fusion(bf16[512,2048]{0,1:T(8,128)(2,1)} %all-gather.11.cloned.1.call-done, bf16[2048,1024]{1,0:T(8,128)(2,1)} %param.20), kind=kOutput, calls=%fused_computation.31 | convolution fusion | flops 2148007936 | bytes 7340032 | tf_op jit(solution)/shard_map/dot_general | solution.py:137
  372.7 7.7 %all-to-all-done.1 = bf16[8,1,64,1024]{3,2,1,0:T(8,128)(2,1)S(1)} async-done(((bf16[8,1,64,1024]{3,2,1,0:T(8,128)(2,1)}), bf16[8,1,64,1024]{3,2,1,0:T(8,128)(2,1)S(1)}, u32[]{:S(2)}, u32[]{:S(2)}) %all-to-all-start.1) | async-done | bytes 1048608 | tf_op jit(solution)/shard_map/all_to_all | solution.py:147
  380.3 1.2 gather_fusion.1
  381.7 2.3 multiply_reduce_fusion
  (68 shorter events, 2.7 us)
Async XLA Ops:
  7.2 23.8 %all-gather.13.cloned.1.call-start = ((), (), s32[]{:S(2)}) async-start(), calls=%async_computation.5 | async-start | bytes 1310720 | tf_op jit(solution)/shard_map/all_gather | solution.py:108
  11.3 87.6 %all-gather.15.cloned.1.call-start = ((), (), s32[]{:S(2)}) async-start(), calls=%async_computation.6 | async-start | bytes 5242880 | tf_op jit(solution)/shard_map/all_gather | solution.py:126
  66.2 107.7 %all-gather.7.cloned.1.call-start = ((), (), s32[]{:S(2)}) async-start(), calls=%async_computation.2 | async-start | bytes 4718592 | tf_op jit(solution)/shard_map/all_gather | solution.py:87
  66.9 180.3 %all-gather.9.cloned.1.call-start = ((), (), s32[]{:S(2)}) async-start(), calls=%async_computation.3 | async-start | bytes 4718592 | tf_op jit(solution)/shard_map/all_gather | solution.py:88
  67.5 208.0 %all-gather.17.cloned.1.call-start = ((), (), s32[]{:S(2)}) async-start(), calls=%async_computation.7 | async-start | bytes 2621440 | tf_op jit(solution)/shard_map/all_gather | solution.py:142
  98.9 5.9 %copy-start.3 = (bf16[1,4096,512]{2,1,0:T(8,128)(2,1)S(1)}, bf16[1,4096,512]{2,1,0:T(8,128)(2,1)}, u32[]{:S(2)}) copy-start(bf16[1,4096,512]{2,1,0:T(8,128)(2,1)} %param.26) | copy-start | bytes 12582916
  98.9 5.9 %copy-start.4 = (bf16[8,1,64,4096]{3,2,0,1:T(8,128)(2,1)S(1)}, bf16[8,1,64,4096]{3,2,0,1:T(8,128)(2,1)}, u32[]{:S(2)}) copy-start(bf16[8,1,64,4096]{3,2,0,1:T(8,128)(2,1)} %all-gather.15.cloned.1.call-done) | copy-start | bytes 12582916
  104.9 3.5 copy-start
  108.1 258.4 %all-gather.11.cloned.1.call-start = ((), (), s32[]{:S(2)}) async-start(), calls=%async_computation.4 | async-start | bytes 2621440 | tf_op jit(solution)/shard_map/all_gather | solution.py:138
  275.5 79.3 %copy-start.1 = (s32[128,2]{0,1:T(2,128)S(1)}, s32[128,2]{0,1:T(2,128)}, u32[]{:S(2)}) copy-start(s32[128,2]{0,1:T(2,128)} %param.23) | copy-start | bytes 3076
  275.5 79.5 %copy-start.2 = (f32[128,2]{0,1:T(2,128)S(1)}, f32[128,2]{0,1:T(2,128)}, u32[]{:S(2)}) copy-start(f32[128,2]{0,1:T(2,128)} %param.24) | copy-start | bytes 3076
  281.7 98.6 %all-to-all-start.1 = ((bf16[8,1,64,1024]{3,2,1,0:T(8,128)(2,1)}), bf16[8,1,64,1024]{3,2,1,0:T(8,128)(2,1)S(1)}, u32[]{:S(2)}, u32[]{:S(2)}) async-start(bf16[8,1,64,1024]{3,2,1,0:T(8,128)(2,1)} %fusion.24), calls=%async_computation.1 | async-start | bytes 2097152 | tf_op jit(solution)/shard_map/all_to_all | solution.py:147
Sparse Core Ops, SparseCore 0:
  11.5 19.4 all-gather.12
  66.3 32.5 all-gather.14
  101.1 72.7 all-gather.6
  175.9 71.3 all-gather.8
  248.6 21.0 all-gather.16
  275.6 90.8 all-gather.10
where the time goes:
time: 392 us; the launch traced here: 391 us
  waiting for transfers between devices  198 us (51%)
  starting transfers between devices  73.3 us (19%)
  blocking collectives  31.5 us (8%)
  local copies, waits for them, and re-layouts  30 us (8%)
  matrix products  25.1 us (6%)
  between operations  14.3 us (4%)
  other arithmetic  11.3 us (3%)
  loops' own time  7.47 us (2%)
    all_to_all x1, starting transfers between devices, body(): lax.all_to_all(leaving, 'ep', split_axis=0, concat_axis=0, tiled=True)  72.9 us
    all_gather x1, waiting for transfers between devices, body(): value_piece = lax.all_gather(values, 'ep', axis=0, tiled=True)  66.9 us
    all_gather x1, waiting for transfers between devices, body(): key_piece = lax.all_gather(key_rows, 'ep', axis=0, tiled=True)  64.3 us
    all_to_all x1, blocking collectives, body(): lax.all_to_all(outgoing, 'ep', split_axis=0, concat_axis=0, tiled=True)  31.5 us
    all_gather x1, waiting for transfers between devices, body(): arrived_rows = lax.all_gather(arrived, 'tp', axis=2, tiled=True)  31.4 us
    all_gather x1, waiting for transfers between devices, body(): group_rows = lax.all_gather(normed, 'tp', axis=0, tiled=True)  14.9 us
    unnamed x16, local copies, waits for them, and re-layouts  14.4 us
    all_gather x1, waiting for transfers between devices, body(): lax.all_gather(attended, 'tp', axis=1, tiled=True)  11.4 us
  transfers between devices with their start and end apart: 7, of which 6 were waited for; matrix products, arithmetic and copies ran while one was open for 14% of the time, Pallas kernels for 0%

commit v1 on v0

--- a/solution.py
+++ b/solution.py
@@ -85,7 +85,12 @@
     )
     state_now = initial
     key_piece = lax.all_gather(key_rows, "ep", axis=0, tiled=True)
-    value_piece = lax.all_gather(values, "ep", axis=0, tiled=True)
+    ring = [values]
+    for hop in range(7):
+        ring.append(lax.ppermute(ring[-1], "ep", [(dev, (dev + 1) % 8) for dev in range(8)]))
+    value_piece = jnp.roll(
+        jnp.concatenate(ring[::-1], axis=0), (lax.axis_index("ep") + 1) * ring[0].shape[0], axis=0
+    )
     shards = key_piece.shape[0] // row_count
     starts = row_count * jnp.arange(shards, dtype=jnp.int32)
     stacked = (

time: 392 us -> 358 us (0.913)
  waiting for transfers between devices: 198 us -> 153 us
  local copies, waits for them, and re-layouts: 30 us -> 40.6 us
    ppermute x0 -> x7, waiting for transfers between devices: none -> 123 us  [body(): lax.ppermute(ring[-1], 'ep', [(dev, (dev + 1) % 8) for dev in range(8)])]
    all_gather x1 -> x0, waiting for transfers between devices: 66.9 us -> none  [body(): value_piece = lax.all_gather(values, 'ep', axis=0, tiled=True)]
    all_gather x1, waiting for transfers between devices: 64.3 us -> 0.01 us  [body(): key_piece = lax.all_gather(key_rows, 'ep', axis=0, tiled=True)]
    all_gather x1, waiting for transfers between devices: 31.4 us -> 0.01 us  [body(): arrived_rows = lax.all_gather(arrived, 'tp', axis=2, tiled=True)]
    unnamed x16 -> x33, local copies, waits for them, and re-layouts: 14.4 us -> 22.8 us
    all_to_all x1, waiting for transfers between devices: 7.67 us -> 3.59 us  [body(): lax.all_to_all(leaving, 'ep', split_axis=0, concat_axis=0, tiled=True)]
  transfers between devices with their start and end apart: 7 -> 13, of which waited for: 6 -> 10; matrix products, arithmetic and copies ran while one was open for 14% -> 18% of each run, Pallas kernels for 0% -> 0%
where the time goes in v1:
time: 358 us; the launch traced here: 356 us
  waiting for transfers between devices  153 us (43%)
  starting transfers between devices  72.8 us (20%)
  local copies, waits for them, and re-layouts  40.6 us (11%)
  blocking collectives  31.5 us (9%)
  matrix products  25.2 us (7%)
  between operations  14.1 us (4%)
  other arithmetic  11.3 us (3%)
  loops' own time  7.53 us (2%)
    ppermute x7, waiting for transfers between devices, body(): lax.ppermute(ring[-1], 'ep', [(dev, (dev + 1) % 8) for dev in range(8)])  123 us
    all_to_all x1, starting transfers between devices, body(): lax.all_to_all(leaving, 'ep', split_axis=0, concat_axis=0, tiled=True)  70.8 us
    all_to_all x1, blocking collectives, body(): lax.all_to_all(outgoing, 'ep', split_axis=0, concat_axis=0, tiled=True)  31.5 us
    unnamed x33, local copies, waits for them, and re-layouts  22.8 us
    all_gather x1, waiting for transfers between devices, body(): group_rows = lax.all_gather(normed, 'tp', axis=0, tiled=True)  14.9 us
    all_gather x1, waiting for transfers between devices, body(): lax.all_gather(attended, 'tp', axis=1, tiled=True)  10.5 us
  transfers between devices with their start and end apart: 13, of which 10 were waited for; matrix products, arithmetic and copies ran while one was open for 18% of the time, Pallas kernels for 0%

profile of v1, /device:TPU:0, one launch (start us, length us, event | category | flops | bytes accessed | tf_op | source)
XLA Modules:
  0.0 355.8 jit_solution(1864054323533965281)
XLA Ops:
  7.2 1.1 convert_reduce_fusion
  8.3 1.2 fusion.49
  9.5 1.8 fusion.51
  11.4 0.8 copy.62
  13.3 0.7 broadcast_multiply_fusion
  14.4 1.4 scatter_custom_fusion
  16.0 14.9 %all-gather.10.cloned.1.call-done = bf16[128,4096]{1,0:T(8,128)(2,1)} async-done(((bf16[32,4096]{1,0:T(8,128)(2,1)}), bf16[128,4096]{1,0:T(8,128)(2,1)}) %all-gather.10.cloned.1.call-update) | async-done | bytes 1048592 | tf_op jit(solution)/shard_map/all_gather | solution.py:113
  30.9 3.6 %gather_fusion = bf16[128,4096]{1,0:T(8,128)(2,1)S(1)} fusion(bf16[128,4096]{1,0:T(8,128)(2,1)} %all-gather.10.cloned.1.call-done, s32[1024]{0:T(1024)S(1)} %pad_clamp_fusion.1), kind=kCustom, calls=%fused_computation | custom fusion | bytes 2097664 | tf_op jit(solution)/shard_map/jit(_take)/gather | solution.py:129
  34.7 31.5 %all_to_all.10 = bf16[8,1,16,4096]{3,2,1,0:T(8,128)(2,1)} all-to-all(bf16[8,1,16,4096]{3,2,1,0:T(8,128)(2,1)S(1)} %broadcast_select_fusion), channel_id=1, replica_groups=mesh['ep'=8,'tp'=4] {'ep'}, dimensions={0} | all-to-all | bytes 2097152 | tf_op jit(solution)/shard_map/all_to_all | solution.py:130
  66.3 0.7 all-gather.6.cloned.1.call-update
  67.0 1.5 collective-permute-start
  68.5 13.9 %collective-permute-done = bf16[512,512]{1,0:T(8,128)(2,1)S(1)} collective-permute-done((bf16[512,512]{1,0:T(8,128)(2,1)S(1)}, bf16[512,512]{1,0:T(8,128)(2,1)S(1)}, u32[]{:S(2)}, u32[]{:S(2)}) %collective-permute-start) | collective-permute-done | bytes 524320 | tf_op jit(solution)/shard_map/ppermute | solution.py:90
  82.4 14.5 %collective-permute-done.1 = bf16[512,512]{1,0:T(8,128)(2,1)S(1)} collective-permute-done((bf16[512,512]{1,0:T(8,128)(2,1)S(1)}, bf16[512,512]{1,0:T(8,128)(2,1)S(1)}, u32[]{:S(2)}, u32[]{:S(2)}) %collective-permute-start.1) | collective-permute-done | bytes 524320 | tf_op jit(solution)/shard_map/ppermute | solution.py:90
  96.8 13.6 %collective-permute-done.2 = bf16[512,512]{1,0:T(8,128)(2,1)S(1)} collective-permute-done((bf16[512,512]{1,0:T(8,128)(2,1)S(1)}, bf16[512,512]{1,0:T(8,128)(2,1)S(1)}, u32[]{:S(2)}, u32[]{:S(2)}) %collective-permute-start.2) | collective-permute-done | bytes 524320 | tf_op jit(solution)/shard_map/ppermute | solution.py:90
  110.5 26.9 %collective-permute-done.3 = bf16[512,512]{1,0:T(8,128)(2,1)S(1)} collective-permute-done((bf16[512,512]{1,0:T(8,128)(2,1)S(1)}, bf16[512,512]{1,0:T(8,128)(2,1)S(1)}, u32[]{:S(2)}, u32[]{:S(2)}) %collective-permute-start.3) | collective-permute-done | bytes 524320 | tf_op jit(solution)/shard_map/ppermute | solution.py:90
  137.4 14.0 %collective-permute-done.4 = bf16[512,512]{1,0:T(8,128)(2,1)S(1)} collective-permute-done((bf16[512,512]{1,0:T(8,128)(2,1)S(1)}, bf16[512,512]{1,0:T(8,128)(2,1)S(1)}, u32[]{:S(2)}, u32[]{:S(2)}) %collective-permute-start.4) | collective-permute-done | bytes 524320 | tf_op jit(solution)/shard_map/ppermute | solution.py:90
  151.4 27.3 %collective-permute-done.5 = bf16[512,512]{1,0:T(8,128)(2,1)} collective-permute-done((bf16[512,512]{1,0:T(8,128)(2,1)S(1)}, bf16[512,512]{1,0:T(8,128)(2,1)}, u32[]{:S(2)}, u32[]{:S(2)}) %collective-permute-start.5) | collective-permute-done | bytes 524320 | tf_op jit(solution)/shard_map/ppermute | solution.py:90
  178.7 6.0 %fusion.27 = f32[8,1,64,512]{3,2,0,1:T(8,128)S(1)} fusion(bf16[1,4096,512]{2,1,0:T(8,128)(2,1)} %param.25, bf16[8,1,64,4096]{3,2,0,1:T(8,128)(2,1)} %all-gather.12.cloned.1.call-done), kind=kOutput, calls=%fused_computation.33 | convolution fusion | flops 2147483648 | bytes 9437184 | tf_op jit(solution)/shard_map/sxcd,xdf->sxcf/dot_general | solution.py:132
  184.7 3.2 fusion.42
  188.2 2.0 copy.57
  190.2 2.0 copy.59
  192.3 0.7 constant_dynamic-slice_fusion.3
  193.0 12.9 %collective-permute-done.6 = bf16[512,512]{1,0:T(8,128)(2,1)} collective-permute-done((bf16[512,512]{1,0:T(8,128)(2,1)}, bf16[512,512]{1,0:T(8,128)(2,1)}, u32[]{:S(2)}, u32[]{:S(2)}) %collective-permute-start.6) | collective-permute-done | bytes 524320 | tf_op jit(solution)/shard_map/ppermute | solution.py:90
  205.9 1.1 constant_dynamic-update-slice_fusion.15
  207.0 1.1 constant_dynamic-update-slice_fusion.14
  208.3 1.1 constant_dynamic-update-slice_fusion.7
  209.4 1.1 constant_dynamic-update-slice_fusion.6
  210.7 2.2 constant_dynamic-slice_fusion.2
  213.0 6.6 %copy.60 = bf16[8,512,512]{1,2,0:T(8,128)(2,1)} copy(bf16[8,512,512]{2,1,0:T(8,128)(2,1)} %bitcast.114) | data formatting | bytes 8388608
  219.6 6.5 %copy.58 = bf16[8,512,512]{1,2,0:T(8,128)(2,1)} copy(bf16[8,512,512]{2,1,0:T(8,128)(2,1)} %bitcast.118) | data formatting | bytes 8388608
  226.2 20.2 %while.16 = (s32[]{:T(128)}, f32[4,512]{1,0:T(4,128)S(1)}, f32[4,512]{1,0:T(4,128)S(1)}, f32[4,512,128]{2,1,0:T(8,128)S(1)}, s32[8]{0:T(128)S(1)}, /*index=5*/s3...) while((s32[]{:T(128)}, f32[4,512]{1,0:T(4,128)S(1)}, ...), condition=%wide.region_5.6_spmd.clone.clone, body=%wide.region_0.5_spmd.clone.clone.sunk | while | flops 555488256 | bytes 19607896 | solution.py:101
  227.5 10.0 %conditional.4 = ((f32[4,512]{1,0:T(4,128)S(1)}, f32[4,512]{1,0:T(4,128)S(1)}, f32[4,512,128]{2,1,0:T(8,128)S(1)})) conditional(s32[]{:T(128)} %convert_element_type.100, (f32[4,512]{1,0:T(4,128)S(1)}, f32[4,512]{1,0:T(4,128)S(1)}, f32[4,512,128]{2,1,0:T(8,128)S(1)}) %tuple.54, (s32[]{:T(128)}, s32[]{:T(128)}, bf16[8,512,512]{1,2,0:T(8,128)(2,1)}, ...), branch_computations={%region_1.1_spmd, %region_2.4_spmd} | conditional | flops 555488256 | bytes 19605586 | solution.py:77
  229.4 0.8 dynamic-slice_bitcast_fusion
  230.2 0.6 iota_add_fusion
  231.1 1.3 constant_dynamic-slice_fusion
  232.4 1.4 fusion.4
  233.8 1.4 fusion.3
  235.2 2.3 fusion.8
  238.8 0.6 dynamic_slice.49
  242.6 0.6 dynamic_slice.49
  246.8 0.9 divide_convert_fusion
  247.8 6.2 %fusion.24 = bf16[8,1,64,1024]{3,2,1,0:T(8,128)(2,1)} fusion(bf16[8,64,2048]{2,1,0:T(8,128)(2,1)} %bitcast.129, bf16[1,2048,1024]{2,1,0:T(8,128)(2,1)} %param.27), kind=kOutput, calls=%fused_computation.32 | convolution fusion | flops 2148007936 | bytes 7340032 | tf_op jit(solution)/shard_map/sxcf,xfd->sxcd/dot_general | solution.py:149
  254.0 70.8 %all-to-all-start.1 = ((bf16[8,1,64,1024]{3,2,1,0:T(8,128)(2,1)}), bf16[8,1,64,1024]{3,2,1,0:T(8,128)(2,1)S(1)}, u32[]{:S(2)}, u32[]{:S(2)}) async-start(bf16[8,1,64,1024]{3,2,1,0:T(8,128)(2,1)} %fusion.24), calls=%async_computation.1 | async-start | bytes 2097152 | tf_op jit(solution)/shard_map/all_to_all | solution.py:152
  325.3 10.5 %all-gather.8.cloned.1.call-done = bf16[512,2048]{0,1:T(8,128)(2,1)} async-done(((bf16[512,512]{0,1:T(8,128)(2,1)}), bf16[512,2048]{0,1:T(8,128)(2,1)}) %all-gather.8.cloned.1.call-update) | async-done | bytes 2097168 | tf_op jit(solution)/shard_map/all_gather | solution.py:143
  335.8 6.1 %convolution_convert_fusion = bf16[512,1024]{1,0:T(8,128)(2,1)} fusion(bf16[512,2048]{0,1:T(8,128)(2,1)} %all-gather.8.cloned.1.call-done, bf16[2048,1024]{1,0:T(8,128)(2,1)} %param.20), kind=kOutput, calls=%fused_computation.31 | convolution fusion | flops 2148007936 | bytes 7340032 | tf_op jit(solution)/shard_map/dot_general | solution.py:142
  341.9 3.6 %all-to-all-done.1 = bf16[8,1,64,1024]{3,2,1,0:T(8,128)(2,1)S(1)} async-done(((bf16[8,1,64,1024]{3,2,1,0:T(8,128)(2,1)}), bf16[8,1,64,1024]{3,2,1,0:T(8,128)(2,1)S(1)}, u32[]{:S(2)}, u32[]{:S(2)}) %all-to-all-start.1) | async-done | bytes 1048608 | tf_op jit(solution)/shard_map/all_to_all | solution.py:152
  345.5 1.2 gather_fusion.1
  346.9 2.3 multiply_reduce_fusion
  (98 shorter events, 7.8 us)
Async XLA Ops:
  7.2 23.8 %all-gather.10.cloned.1.call-start = ((), (), s32[]{:S(2)}) async-start(), calls=%async_computation.4 | async-start | bytes 1310720 | tf_op jit(solution)/shard_map/all_gather | solution.py:113
  11.3 167.3 %all-gather.12.cloned.1.call-start = ((), (), s32[]{:S(2)}) async-start(), calls=%async_computation.5 | async-start | bytes 5242880 | tf_op jit(solution)/shard_map/all_gather | solution.py:131
  34.5 32.5 %copy-start = (bf16[512,512]{1,0:T(8,128)(2,1)S(1)}, bf16[512,512]{1,0:T(8,128)(2,1)}, u32[]{:S(2)}) copy-start(bf16[512,512]{1,0:T(8,128)(2,1)} %param.18) | copy-start | bytes 1572868
  66.2 153.4 %all-gather.6.cloned.1.call-start = ((), (), s32[]{:S(2)}) async-start(), calls=%async_computation.2 | async-start | bytes 4718592 | tf_op jit(solution)/shard_map/all_gather | solution.py:87
  66.9 180.8 %all-gather.14.cloned.1.call-start = ((), (), s32[]{:S(2)}) async-start(), calls=%async_computation.6 | async-start | bytes 2621440 | tf_op jit(solution)/shard_map/all_gather | solution.py:147
  67.0 15.4 %collective-permute-start = (bf16[512,512]{1,0:T(8,128)(2,1)S(1)}, bf16[512,512]{1,0:T(8,128)(2,1)S(1)}, u32[]{:S(2)}, u32[]{:S(2)}) collective-permute-start(bf16[512,512]{1,0:T(8,128)(2,1)S(1)} %copy-done), channel_id=1, source_target_pairs={{0,4},{4,8},{8,12},{12,16},{16,20},{20,24},{24,28},{28,0},{1,5},{5... | collective-permute-start | bytes 1572872 | tf_op jit(solution)/shard_map/ppermute | solution.py:90
  82.4 14.5 %collective-permute-start.1 = (bf16[512,512]{1,0:T(8,128)(2,1)S(1)}, bf16[512,512]{1,0:T(8,128)(2,1)S(1)}, u32[]{:S(2)}, u32[]{:S(2)}) collective-permute-start(bf16[512,512]{1,0:T(8,128)(2,1)S(1)} %collective-permute-done), channel_id=1, source_target_pairs={{0,4},{4,8},{8,12},{12,16},{16,20},{20,24},{24,28},{28,0},{1,5},{5... | collective-permute-start | bytes 1572872 | tf_op jit(solution)/shard_map/ppermute | solution.py:90
  96.8 13.6 %collective-permute-start.2 = (bf16[512,512]{1,0:T(8,128)(2,1)S(1)}, bf16[512,512]{1,0:T(8,128)(2,1)S(1)}, u32[]{:S(2)}, u32[]{:S(2)}) collective-permute-start(bf16[512,512]{1,0:T(8,128)(2,1)S(1)} %collective-permute-done.1), channel_id=1, source_target_pairs={{0,4},{4,8},{8,12},{12,16},{16,20},{20,24},{24,28},{28,0},{1,5},{5... | collective-permute-start | bytes 1572872 | tf_op jit(solution)/shard_map/ppermute | solution.py:90
  110.4 26.9 %collective-permute-start.3 = (bf16[512,512]{1,0:T(8,128)(2,1)S(1)}, bf16[512,512]{1,0:T(8,128)(2,1)S(1)}, u32[]{:S(2)}, u32[]{:S(2)}) collective-permute-start(bf16[512,512]{1,0:T(8,128)(2,1)S(1)} %collective-permute-done.2), channel_id=1, source_target_pairs={{0,4},{4,8},{8,12},{12,16},{16,20},{20,24},{24,28},{28,0},{1,5},{5... | collective-permute-start | bytes 1572872 | tf_op jit(solution)/shard_map/ppermute | solution.py:90
  137.4 14.0 %collective-permute-start.4 = (bf16[512,512]{1,0:T(8,128)(2,1)S(1)}, bf16[512,512]{1,0:T(8,128)(2,1)S(1)}, u32[]{:S(2)}, u32[]{:S(2)}) collective-permute-start(bf16[512,512]{1,0:T(8,128)(2,1)S(1)} %collective-permute-done.3), channel_id=1, source_target_pairs={{0,4},{4,8},{8,12},{12,16},{16,20},{20,24},{24,28},{28,0},{1,5},{5... | collective-permute-start | bytes 1572872 | tf_op jit(solution)/shard_map/ppermute | solution.py:90
  151.4 27.3 %collective-permute-start.5 = (bf16[512,512]{1,0:T(8,128)(2,1)S(1)}, bf16[512,512]{1,0:T(8,128)(2,1)}, u32[]{:S(2)}, u32[]{:S(2)}) collective-permute-start(bf16[512,512]{1,0:T(8,128)(2,1)S(1)} %collective-permute-done.4), channel_id=1, source_target_pairs={{0,4},{4,8},{8,12},{12,16},{16,20},{20,24},{24,28},{28,0},{1,5},{5... | collective-permute-start | bytes 1572872 | tf_op jit(solution)/shard_map/ppermute | solution.py:90
  178.7 27.2 %collective-permute-start.6 = (bf16[512,512]{1,0:T(8,128)(2,1)}, bf16[512,512]{1,0:T(8,128)(2,1)}, u32[]{:S(2)}, u32[]{:S(2)}) collective-permute-start(bf16[512,512]{1,0:T(8,128)(2,1)} %collective-permute-done.5), channel_id=1, source_target_pairs={{0,4},{4,8},{8,12},{12,16},{16,20},{20,24},{24,28},{28,0},{1,5},{5... | collective-permute-start | bytes 1572872 | tf_op jit(solution)/shard_map/ppermute | solution.py:90
  178.7 6.0 %copy-start.4 = (bf16[1,4096,512]{2,1,0:T(8,128)(2,1)S(1)}, bf16[1,4096,512]{2,1,0:T(8,128)(2,1)}, u32[]{:S(2)}) copy-start(bf16[1,4096,512]{2,1,0:T(8,128)(2,1)} %param.26) | copy-start | bytes 12582916
  178.7 6.0 %copy-start.5 = (bf16[8,1,64,4096]{3,2,0,1:T(8,128)(2,1)S(1)}, bf16[8,1,64,4096]{3,2,0,1:T(8,128)(2,1)}, u32[]{:S(2)}) copy-start(bf16[8,1,64,4096]{3,2,0,1:T(8,128)(2,1)} %all-gather.12.cloned.1.call-done) | copy-start | bytes 12582916
  187.9 147.9 %all-gather.8.cloned.1.call-start = ((), (), s32[]{:S(2)}) async-start(), calls=%async_computation.3 | async-start | bytes 2621440 | tf_op jit(solution)/shard_map/all_gather | solution.py:143
  219.6 6.6 %copy-start.1 = (bf16[512,4,128]{2,0,1:T(8,128)(2,1)S(1)}, bf16[512,4,128]{2,0,1:T(8,128)(2,1)}, u32[]{:S(2)}) copy-start(bf16[512,4,128]{2,0,1:T(8,128)(2,1)} %copy.59) | copy-start | bytes 1572868
  247.8 77.2 %copy-start.2 = (s32[128,2]{0,1:T(2,128)S(1)}, s32[128,2]{0,1:T(2,128)}, u32[]{:S(2)}) copy-start(s32[128,2]{0,1:T(2,128)} %param.23) | copy-start | bytes 3076
  247.8 77.4 %copy-start.3 = (f32[128,2]{0,1:T(2,128)S(1)}, f32[128,2]{0,1:T(2,128)}, u32[]{:S(2)}) copy-start(f32[128,2]{0,1:T(2,128)} %param.24) | copy-start | bytes 3076
  254.0 91.6 %all-to-all-start.1 = ((bf16[8,1,64,1024]{3,2,1,0:T(8,128)(2,1)}), bf16[8,1,64,1024]{3,2,1,0:T(8,128)(2,1)S(1)}, u32[]{:S(2)}, u32[]{:S(2)}) async-start(bf16[8,1,64,1024]{3,2,1,0:T(8,128)(2,1)} %fusion.24), calls=%async_computation.1 | async-start | bytes 2097152 | tf_op jit(solution)/shard_map/all_to_all | solution.py:152
Sparse Core Ops, SparseCore 0:
  11.5 19.4 all-gather.9
  66.3 32.5 all-gather.11
  101.1 99.7 all-gather.5
  202.3 27.2 all-gather.13
  247.9 87.8 all-gather.7
